TPU v7x, 32 devices: a whole 2x2x4 slice. The times are simulated.
32 devices in a mesh: grp: 2 (over y), dp: 2 (over x), kv: 4 (over z), tp: 2 (over core).
Axes of the slice: x: 2, y: 2, z: 4, core: 2. Of those that a mesh axis runs over, the one named last changes fastest.
Arguments:
- hidden_in: bfloat16 [4, 1024, 2048], P(('grp', 'dp'), 'kv', 'tp'), parts along dimension 0, may hold values from -45 to 45
- norm_gain: float32 [2048], P('tp'), may hold values from 0.1 to 1.9
- query_weight: bfloat16 [2048, 1024], P('kv', 'tp'), may hold values from -1 to 1
- key_weight: bfloat16 [2048, 256], P('kv', 'tp'), may hold values from -60 to 60
- value_weight: bfloat16 [2048, 256], P('kv', 'tp'), may hold values from -0.125 to 0.125
- out_weight: bfloat16 [2048, 1024], P('kv', 'tp'), may hold values from -0.1875 to 0.1875
- slopes: float32 [8], P('tp'), may hold values from 0 to 3
- block_choice: int32 [4, 16, 16], P(('grp', 'dp'), 'kv'), parts along dimension 0, may hold values from 0 to 15, as said below
Outputs:
- mixed: bfloat16 [4, 1024, 2048], P(('grp', 'dp'), ('kv', 'tp')), parts along dimension 0
There are 2 independent parts, one for each index of `grp`. A program takes and returns all parts, laid end to end along the dimension named above; an argument that names none is the same for every part. Nothing has to cross between parts.
Inputs may be any that keep to these rules, and one draw needn't show every extreme that they name: `block_choice`: for query block i the entries name key blocks 0 to i; the first min(16, i + 1) entries are distinct and include block i; any later entries equal i.
All inputs are finite; a program needn't handle non-finite values.
Results may differ from a plain program's by a relative error of at most 0.0092.
Values may be sent and summed in bfloat16 or wider, within the bound.
A program may use at most 64 MiB of HBM per device.

v0:
```python
import jax
import jax.numpy as jnp
from jax import lax
from jax.sharding import PartitionSpec as P

D = 2048
HEAD_DIM = 128
BLOCK = 64
NSEL = 16


EPS = 1e-06
NEG = -1e30


def project(rows, weight):
    return jnp.dot(rows, weight, preferred_element_type=jnp.float32)


def on_device(
    hidden_in, norm_gain, query_weight, key_weight, value_weight, out_weight, slopes, block_choice
):
    tokens = hidden_in.shape[1]
    local = hidden_in[0].astype(jnp.float32)
    square_sum = lax.psum(jnp.sum(local * local, axis=1), "tp")
    scaled = local * lax.rsqrt(square_sum / D + EPS)[:, None] * norm_gain[None, :]
    normed = scaled.astype(jnp.bfloat16)
    rows = lax.all_gather(normed, "tp", axis=1, tiled=True)
    pieces = (
        lax.all_gather(query_weight, "kv", axis=0, tiled=True),
        lax.all_gather(key_weight, "kv", axis=0, tiled=True),
        lax.all_gather(value_weight, "kv", axis=0, tiled=True),
    )
    query_acc, key_acc, value_acc = tuple((project(rows, piece) for piece in pieces))
    queries = query_acc.astype(jnp.bfloat16)
    keys = key_acc.astype(jnp.bfloat16)
    values = value_acc.astype(jnp.bfloat16)
    head_local = query_weight.shape[1] // HEAD_DIM
    kv_local = key_weight.shape[1] // HEAD_DIM
    group = head_local // kv_local
    query_four = queries.reshape(tokens, kv_local, group, HEAD_DIM)
    slope_grid = slopes.reshape(kv_local, group)
    offset = lax.axis_index("kv") * tokens
    qpos = offset + jnp.arange(tokens, dtype=jnp.int32)
    choice_local = block_choice[0]
    local_blocks = choice_local.shape[0]
    scale = HEAD_DIM ** (-0.5)
    key_all, value_all = (
        lax.all_gather(keys, "kv", axis=0, tiled=True),
        lax.all_gather(values, "kv", axis=0, tiled=True),
    )
    key_sel = key_all.reshape(-1, BLOCK, kv_local, HEAD_DIM)[choice_local]
    value_sel = value_all.reshape(-1, BLOCK, kv_local, HEAD_DIM)[choice_local]
    key_sel = key_sel.reshape(local_blocks, NSEL * BLOCK, kv_local, HEAD_DIM)
    value_sel = value_sel.reshape(local_blocks, NSEL * BLOCK, kv_local, HEAD_DIM)
    query_blocks = query_four.reshape(local_blocks, BLOCK, kv_local, group, HEAD_DIM)
    scores = (
        jnp.einsum("nqkgd,nskd->nqkgs", query_blocks, key_sel, preferred_element_type=jnp.float32)
        * scale
    )
    kpos = (
        choice_local[:, :, None] * BLOCK + jnp.arange(BLOCK, dtype=jnp.int32)[None, None, :]
    ).reshape(local_blocks, NSEL * BLOCK)
    qpos_blocks = qpos.reshape(local_blocks, BLOCK)
    dist = jnp.abs(qpos_blocks[:, :, None] - kpos[:, None, :]).astype(jnp.float32) / BLOCK
    scores = scores - slope_grid[None, None, :, :, None] * dist[:, :, None, None, :]
    global_block = offset // BLOCK + jnp.arange(local_blocks, dtype=jnp.int32)
    live = jnp.arange(NSEL, dtype=jnp.int32)[None, :] < jnp.minimum(NSEL, global_block + 1)[:, None]
    live = jnp.repeat(live, BLOCK, axis=1)[:, None, None, None, :]
    scores = jnp.where(live, scores, NEG)
    best = jnp.max(scores, axis=4, keepdims=True)
    weights = jnp.where(live, jnp.exp(scores - best), 0.0)
    total = jnp.sum(weights, axis=4)
    summed = jnp.einsum(
        "nqkgs,nskd->nqkgd",
        weights.astype(jnp.bfloat16),
        value_sel,
        preferred_element_type=jnp.float32,
    )
    attended = (
        (summed / total[..., None]).astype(jnp.bfloat16).reshape(tokens, head_local * HEAD_DIM)
    )
    out_full = lax.all_gather(out_weight, "kv", axis=0, tiled=True)
    piece = attended
    mixed = lax.psum_scatter(
        lax.dot_general(
            piece, out_full, (((1,), (1,)), ((), ())), preferred_element_type=jnp.float32
        ).astype(jnp.bfloat16),
        "tp",
        scatter_dimension=0,
        tiled=True,
    )
    return mixed[None]


def solution(mesh):
    in_specs = (
        P(("grp", "dp"), "kv", "tp"),
        P("tp"),
        P("kv", "tp"),
        P("kv", "tp"),
        P("kv", "tp"),
        P("kv", "tp"),
        P("tp"),
        P(("grp", "dp"), "kv", None),
    )
    out_specs = P(("grp", "dp"), ("kv", "tp"), None)
    return jax.shard_map(
        on_device, mesh=mesh, in_specs=in_specs, out_specs=out_specs, check_vma=False
    )
```

profile of v0, /device:TPU:25, one launch (start us, length us, event | category | flops | bytes accessed | tf_op | source)
XLA Modules:
  0.0 149.4 jit_solution(17970250858002666095)
XLA Ops:
  6.5 1.2 fusion.10
  7.8 2.8 %psum.7 = f32[256]{0:T(256)S(1)} all-reduce(f32[256]{0:T(256)S(1)} %fusion.10), channel_id=1, replica_groups=mesh['grp'=2,'dp'=2,'kv'=4,'tp'=2] {'tp'}, use_global_device_ids=true, to_apply=%region_1.0 | all-reduce | flops 256 | bytes 2048 | tf_op jit(solution)/shard_map/psum | solution.py:25
  10.6 2.0 %fusion.12 = bf16[256,1024]{1,0:T(8,128)(2,1)} fusion(bf16[1,256,1024]{2,1,0:T(8,128)(2,1)} %param.8, f32[1024]{0:T(1024)} %param.9, f32[256]{0:T(256)S(1)} %add_rsqrt_fusion), kind=kLoop, calls=%fused_computation.19 | loop fusion | flops 1048576 | bytes 1053696 | tf_op jit(solution)/shard_map/convert_element_type | solution.py:27
  12.7 0.7 all-gather.6.cloned.1.call-update
  13.4 0.7 all-gather.8.cloned.1.call-update
  14.2 0.7 multiply_bitcast_fusion
  14.9 0.7 compare_select_fusion
  15.6 13.4 %all_gather.24 = bf16[2048,128]{1,0:T(8,128)(2,1)S(1)} all-gather(bf16[512,128]{1,0:T(8,128)(2,1)} %param.11), channel_id=1, replica_groups=mesh['grp'=2,'dp'=2,'kv'=4,'tp'=2] {'kv'}, dimensions={0}, use_global_device_ids=true | all-gather | bytes 655360 | tf_op jit(solution)/shard_map/all_gather | solution.py:31
  29.0 20.1 %all_gather.22 = bf16[2048,128]{1,0:T(8,128)(2,1)S(1)} all-gather(bf16[512,128]{1,0:T(8,128)(2,1)} %param.12), channel_id=1, replica_groups=mesh['grp'=2,'dp'=2,'kv'=4,'tp'=2] {'kv'}, dimensions={0}, use_global_device_ids=true | all-gather | bytes 655360 | tf_op jit(solution)/shard_map/all_gather | solution.py:32
  49.6 0.3 convert_multiply_fusion.2
  50.0 1.7 %convolution_convert_fusion.2 = bf16[256,128]{1,0:T(8,128)(2,1)S(1)} fusion(bf16[256,2048]{1,0:T(8,128)(2,1)} %all-gather.4.cloned.1.call-done, bf16[2048,128]{1,0:T(8,128)(2,1)S(1)} %all_gather.24), kind=kOutput, calls=%fused_computation.15 | convolution fusion | flops 134250496 | bytes 1638400 | tf_op jit(solution)/shard_map/dot_general | solution.py:17
  51.7 13.8 %all_gather.25 = bf16[1024,128]{1,0:T(8,128)(2,1)S(1)} all-gather(bf16[256,128]{1,0:T(8,128)(2,1)S(1)} %convolution_convert_fusion.2), channel_id=1, replica_groups=mesh['grp'=2,'dp'=2,'kv'=4,'tp'=2] {'kv'}, dimensions={0}, use_global_device_ids=true | all-gather | bytes 327680 | tf_op jit(solution)/shard_map/all_gather | solution.py:49
  65.5 1.7 %gather_fusion.1 = bf16[64,64,128]{2,1,0:T(8,128)(2,1)} fusion(bf16[16,64,128]{2,1,0:T(8,128)(2,1)S(1)} %bitcast.83, s32[1024]{0:T(1024)S(1)} %pad_clamp_fusion), kind=kCustom, calls=%fused_computation.1 | custom fusion | bytes 2097408 | tf_op jit(solution)/shard_map/gather | solution.py:52
  67.2 0.4 convolution_convert_fusion.3
  67.7 13.4 %all_gather.23 = bf16[1024,128]{1,0:T(8,128)(2,1)S(1)} all-gather(bf16[256,128]{1,0:T(8,128)(2,1)S(1)} %convolution_convert_fusion.3), channel_id=1, replica_groups=mesh['grp'=2,'dp'=2,'kv'=4,'tp'=2] {'kv'}, dimensions={0}, use_global_device_ids=true | all-gather | bytes 327680 | tf_op jit(solution)/shard_map/all_gather | solution.py:50
  81.1 0.7 gather_fusion
  81.9 1.4 all-gather.6.cloned.1.call-done
  83.3 2.3 %convolution_convert_fusion.1 = bf16[256,512]{1,0:T(8,128)(2,1)S(1)} fusion(bf16[256,2048]{1,0:T(8,128)(2,1)S(1)} %copy-done, bf16[2048,512]{1,0:T(8,128)(2,1)} %all-gather.6.cloned.1.call-done), kind=kOutput, calls=%fused_computation.14 | convolution fusion | flops 537001984 | bytes 3407872 | tf_op jit(solution)/shard_map/dot_general | solution.py:17
  85.6 2.3 %fusion.3 = (f32[4,64,4]{1,2,0:T(4,128)S(1)}, f32[4,1024,64,4]{1,2,3,0:T(8,128)S(1)}) fusion(f32[4,64,1024]{2,1,0:T(8,128)S(1)} %convert_multiply_fusion.2, f32[4]{0:T(128)S(1)} %copy-done.1, pred[4,1024]{1,0:T(4,128)(4,1)S(1)} %broadcast_in_dim.37, bf16[4,1024,128,1]{2,1,3,0:T(8,128)(2,1)} %bitcast.85, bf16[4,64,4,128]{3,2,1,0:T(4,128)(2,1)S(1)} %reshape.129), kind=kOutput, calls=%fused_computation.8 | convolution fusion | flops 273677312 | bytes 6561808 | tf_op jit(solution)/shard_map/nqkgd,nskd->nqkgs/dot_general | solution.py:58
  88.0 1.5 fusion.1
  89.4 1.6 %fusion.19 = bf16[4,64,1,4,128]{4,1,3,0,2:T(8,128)(2,1)S(1)} fusion(bf16[4,1024,128,1]{2,1,3,0:T(8,128)(2,1)S(1)} %bitcast.84, f32[4,1024,64,4]{1,2,3,0:T(8,128)S(1)} %get-tuple-element.6, f32[4,64,4]{1,2,0:T(4,128)S(1)} %get-tuple-element.5, f32[4,64,1024]{2,1,0:T(8,128)S(1)} %convert_multiply_fusion.2, f32[4]{0:T(128)S(1)} %copy-done.1, ...), kind=kOutput, calls=%fused_computation.23 | convolution fusion | flops 276037632 | bytes 6565904 | tf_op jit(solution)/shard_map/nqkgs,nskd->nqkgd/dot_general | solution.py:74
  91.3 38.4 %all-gather.8.cloned.1.call-done = bf16[2048,512]{1,0:T(8,128)(2,1)} async-done(((bf16[512,512]{1,0:T(8,128)(2,1)}), bf16[2048,512]{1,0:T(8,128)(2,1)}) %all-gather.8.cloned.1.call-update) | async-done | bytes 2097168 | tf_op jit(solution)/shard_map/all_gather | solution.py:83
  129.6 3.3 %convolution_convert_fusion = bf16[256,2048]{1,0:T(8,128)(2,1)} fusion(bf16[2048,512]{1,0:T(8,128)(2,1)} %all-gather.8.cloned.1.call-done, bf16[32,8,4,128]{3,2,1,0:T(4,128)(2,1)S(1)} %bitcast.86), kind=kOutput, calls=%fused_computation.7 | convolution fusion | flops 537395200 | bytes 3407872 | tf_op jit(solution)/shard_map/dot_general | solution.py:86
  133.0 9.8 %reduce-scatter.2.cloned.1.call-done = bf16[128,2048]{1,0:T(8,128)(2,1)} async-done(((bf16[256,2048]{1,0:T(8,128)(2,1)}), bf16[128,2048]{1,0:T(8,128)(2,1)}) %reduce-scatter.2.cloned.1.call-update) | async-done | bytes 524304 | tf_op jit(solution)/shard_map/reduce_scatter | solution.py:85
  (26 shorter events, 1.0 us)
Async XLA Ops:
  6.5 43.4 %all-gather.4.cloned.1.call-start = ((), (), s32[]{:S(2)}) async-start(), calls=%async_computation.1 | async-start | bytes 1572864 | tf_op jit(solution)/shard_map/all_gather | solution.py:28
  12.6 70.6 %all-gather.6.cloned.1.call-start = ((), (), s32[]{:S(2)}) async-start(), calls=%async_computation.2 | async-start | bytes 2621440 | tf_op jit(solution)/shard_map/all_gather | solution.py:30
  13.4 116.3 %all-gather.8.cloned.1.call-start = ((), (), s32[]{:S(2)}) async-start(), calls=%async_computation.3 | async-start | bytes 2621440 | tf_op jit(solution)/shard_map/all_gather | solution.py:83
  14.1 128.7 %reduce-scatter.2.cloned.1.call-start = ((), (), s32[]{:S(2)}) async-start(), calls=%async_computation.4 | async-start | bytes 1572864 | tf_op jit(solution)/shard_map/reduce_scatter | solution.py:85
  49.9 17.3 %copy-start = (bf16[256,2048]{1,0:T(8,128)(2,1)S(1)}, bf16[256,2048]{1,0:T(8,128)(2,1)}, u32[]{:S(2)}) copy-start(bf16[256,2048]{1,0:T(8,128)(2,1)} %all-gather.4.cloned.1.call-done) | copy-start | bytes 3145732
  67.2 18.4 %copy-start.1 = (f32[4]{0:T(128)S(1)}, f32[4]{0:T(128)}, u32[]{:S(2)}) copy-start(f32[4]{0:T(128)} %param.14) | copy-start | bytes 52
Sparse Core Ops, SparseCore 0:
  12.7 10.3 all-gather.3
  24.7 58.4 all-gather.5
  84.8 44.7 all-gather.7
  133.1 9.6 reduce-scatter.1
where the time goes:
time: 151 us; the launch traced here: 149 us
  blocking collectives  63.6 us (42%)
  waiting for transfers between devices  51.1 us (34%)
  between operations  13.2 us (9%)
  matrix products  11.7 us (8%)
  other arithmetic  6.49 us (4%)
  local copies, waits for them, and re-layouts  3.2 us (2%)
    all_gather x1, waiting for transfers between devices, on_device(): out_full = lax.all_gather(out_weight, 'kv', axis=0, tiled=True)  38.4 us
    all_gather x1, blocking collectives, on_device(): lax.all_gather(value_weight, 'kv', axis=0, tiled=True)  20.1 us
    all_gather x1, blocking collectives, on_device(): lax.all_gather(keys, 'kv', axis=0, tiled=True)  13.8 us
    all_gather x1, blocking collectives, on_device(): lax.all_gather(key_weight, 'kv', axis=0, tiled=True)  13.4 us
    all_gather x1, blocking collectives, on_device(): lax.all_gather(values, 'kv', axis=0, tiled=True)  13.4 us
    reduce_scatter x1, waiting for transfers between devices, on_device(): lax.psum_scatter(lax.dot_general(piece, out_full, (((1,), (1,)), ((), ())...  9.84 us
    dot_general x3, matrix products, project(): return jnp.dot(rows, weight, preferred_element_type=jnp.float32)  4.45 us
    dot_general x1, matrix products, on_device(): lax.dot_general(piece, out_full, (((1,), (1,)), ((), ())), preferred_elem...  3.33 us
  transfers between devices with their start and end apart: 4, of which 3 were waited for; matrix products, arithmetic and copies ran while one was open for 10% of the time, Pallas kernels for 0%

commit v1 on v0

v1 whole, which is shorter than its diff:
```python
import functools

import jax
import jax.numpy as jnp
from jax import lax
from jax.experimental import pallas as pl
from jax.experimental.pallas import tpu as pltpu
from jax.sharding import PartitionSpec as P

HEAD_DIM = 128
BLOCK = 64
NSEL = 16
EPS = 1e-06
NEG = -1e30
MESH = pl.DeviceIdType.MESH
BF16 = jnp.bfloat16
F32 = jnp.float32


def dot(a, b):
    return jnp.dot(a, b, preferred_element_type=F32)


def dot_t(a, b):
    return lax.dot_general(a, b, (((1,), (1,)), ((), ())), preferred_element_type=F32)


def loop(low, high, body):
    if high - low <= 4:
        for i in range(low, high):
            body(i)
    else:
        lax.fori_loop(low, high, lambda i, c: (body(i), c)[1], 0)


def kernel(n, masked, *refs):
    refs = list(refs)
    hid, gain, wq, wk, wv, wo, slopes = refs[:7]
    refs = refs[7:]
    mask = refs.pop(0) if masked else None
    (
        out, hid2, gain2, xn, fq, fk, fv, fo, qacc, kacc, vacc, qs, kall, vall,
        mrun, lrun, acc, att, pown, psend, precv,
        wsend, wrecv, ksend, krecv, hsend, hrecv, osend, orecv,
    ) = refs
    grp, dp = lax.axis_index("grp"), lax.axis_index("dp")
    z, tp = lax.axis_index("kv"), lax.axis_index("tp")
    xb, yb = lax.rem(dp, 2), lax.rem(grp, 2)
    col = 2 * yb + xb
    col_x, col_y, col_d = 2 * yb + 1 - xb, 2 * (1 - yb) + xb, 2 * (1 - yb) + 1 - xb
    x_id = (grp, dp + 1 - 2 * xb, z, tp)
    y_id = (grp + 1 - 2 * yb, dp, z, tp)
    sib = (grp, dp, z, 1 - tp)

    def at_z(other):
        return (grp, dp, other, tp)

    tokens, half_d = hid.shape
    heads = slopes.shape[0]
    rows = xn.shape[2]
    groups = (((wk, fk, 0), (wv, fv, 1)), ((wq, fq, 2),), ((wo, fo, 3),))

    barrier = pltpu.get_barrier_semaphore()
    for dev in (sib, x_id, y_id):
        pl.semaphore_signal(barrier, inc=1, device_id=dev, device_id_type=MESH)
    for d in range(1, n):
        pl.semaphore_signal(barrier, inc=1, device_id=at_z(lax.rem(z + d, n)), device_id_type=MESH)
    pl.semaphore_wait(barrier, n + 2)

    def remote(src, dst, send, recv, dev):
        return pltpu.make_async_remote_copy(
            src_ref=src, dst_ref=dst, send_sem=send, recv_sem=recv, device_id=dev, device_id_type=MESH
        )

    swap = [
        remote(hid, hid2, hsend.at[0], hrecv.at[0], sib),
        remote(gain, gain2, hsend.at[1], hrecv.at[1], sib),
    ]
    for copy in swap:
        copy.start()

    def along(shard, origin, kind, own):
        w, f, a = shard
        part = pl.ds(2 * col, 2)
        src = w.at[part] if own else f.at[origin, part]
        dev = at_z(z + 1) if kind == 0 else at_z(z - 1)
        return remote(src, f.at[origin, part], wsend.at[a, kind, origin], wrecv.at[a, 0, origin], dev)

    def across(shard, origin, kind):
        _, f, a = shard
        part, dev = {
            2: (pl.ds(2 * col, 2), x_id),
            3: (pl.ds(2 * col, 2), y_id),
            4: (pl.ds(2 * col_x, 1), y_id),
            5: (pl.ds(2 * col_y + 1, 1), x_id),
        }[kind]
        ref = f.at[origin, part]
        return remote(ref, ref, wsend.at[a, kind, origin], wrecv.at[a, kind, origin], dev)

    def arrive(shard, origin, kind):
        _, f, a = shard
        part = {
            0: pl.ds(2 * col, 2),
            2: pl.ds(2 * col_x, 2),
            3: pl.ds(2 * col_y, 2),
            4: pl.ds(2 * col_d, 1),
            5: pl.ds(2 * col_d + 1, 1),
        }[kind]
        ref = f.at[origin, part]
        remote(ref, ref, wsend.at[a, kind, origin], wrecv.at[a, kind, origin], x_id).wait_recv()

    def start_own(g):
        for shard in groups[g]:
            @pl.when(z + 1 < n)
            def _():
                along(shard, z, 0, True).start()

            @pl.when(z >= 1)
            def _():
                along(shard, z, 1, True).start()

    def both(d, body):
        @pl.when(z - d >= 0)
        def _():
            body(z - d, True)

        @pl.when(z + d < n)
        def _():
            body(z + d, False)

    def step_a(g, d):
        def body(origin, up):
            for shard in groups[g]:
                arrive(shard, origin, 0)
                if up:
                    @pl.when(z + 1 < n)
                    def _():
                        along(shard, origin, 0, False).start()
                else:
                    @pl.when(z >= 1)
                    def _():
                        along(shard, origin, 1, False).start()
                across(shard, origin, 2).start()
                across(shard, origin, 3).start()

        both(d, body)

    def step_b(g, d):
        def body(origin, up):
            for shard in groups[g]:
                arrive(shard, origin, 2)
                across(shard, origin, 4).start()
                arrive(shard, origin, 3)
                across(shard, origin, 5).start()

        both(d, body)

    def whole(f, origin):
        return f[origin].reshape(rows, f.shape[-1])

    def step_c(g, d):
        def body(origin, up):
            for shard in groups[g]:
                arrive(shard, origin, 4)
                arrive(shard, origin, 5)
                if g < 2:
                    target = (kacc, vacc, qacc)[shard[2]]
                    target[...] += dot(xn[origin], whole(shard[1], origin))
                else:
                    project_out(origin, whole(fo, origin))

        both(d, body)

    start_own(0)
    start_own(1)

    for copy in swap:
        copy.wait()
    lanes = HEAD_DIM
    square = jnp.zeros((tokens, lanes), F32)
    for ref in (hid, hid2):
        for j in range(half_d // lanes):
            piece = ref[:, j * lanes : (j + 1) * lanes].astype(F32)
            square = square + piece * piece
    inverse = lax.rsqrt(jnp.sum(square, axis=1, keepdims=True) / (2 * half_d) + EPS)
    for ref, g_ref, half in ((hid, gain, tp), (hid2, gain2, 1 - tp)):
        for j in range(half_d // lanes):
            piece = ref[:, j * lanes : (j + 1) * lanes].astype(F32)
            value = (piece * inverse * g_ref[j : j + 1, :]).astype(BF16)
            first = j * lanes
            xn[half * (n // 2) + first // rows, :, first % rows : first % rows + lanes] = value

    mine = xn[z]
    kacc[...] = dot(mine, wk[...].reshape(rows, -1))
    vacc[...] = dot(mine, wv[...].reshape(rows, -1))
    qacc[...] = dot(mine, wq[...].reshape(rows, -1))

    def key_copy(ref, i, d):
        return remote(ref.at[z], ref.at[z], ksend.at[i, d], krecv.at[i, z], at_z(z + d))

    def key_each(d, act):
        @pl.when(z + d < n)
        def _():
            for i, ref in enumerate((kall, vall)):
                act(key_copy(ref, i, d))

    def pipe(d):
        step_a(0, d)
        if isinstance(d, int):
            if d > 1:
                step_b(0, d - 1)
            if d > 2:
                step_c(0, d - 2)
        else:
            pl.when(d > 1)(lambda: step_b(0, d - 1))
            pl.when(d > 2)(lambda: step_c(0, d - 2))

    loop(1, n, pipe)
    step_a(1, 1)
    step_b(0, n - 1)
    step_c(0, n - 2)
    step_a(1, 2)
    step_b(1, 1)
    step_c(0, n - 1)
    kall[z] = kacc[...].astype(BF16)
    vall[z] = vacc[...].astype(BF16)
    loop(1, n, lambda d: key_each(d, lambda copy: copy.start()))
    start_own(2)

    def pipe_q(d):
        step_a(1, d)
        step_b(1, d - 1)
        step_c(1, d - 2)

    loop(3, n, pipe_q)
    step_b(1, n - 1)
    step_c(1, n - 2)
    step_c(1, n - 1)
    for h in range(heads):
        qs[h] = qacc[:, h * HEAD_DIM : (h + 1) * HEAD_DIM].astype(BF16)

    scale = HEAD_DIM**-0.5
    qpos = lax.broadcasted_iota(jnp.int32, (tokens, tokens), 0)
    kpos = lax.broadcasted_iota(jnp.int32, (tokens, tokens), 1)

    def chunk(d, first):
        origin = z - d
        if not first:
            for i, ref in enumerate((kall, vall)):
                remote(ref.at[origin], ref.at[origin], ksend.at[i, d], krecv.at[i, origin], sib).wait_recv()
        keys, values = kall[origin], vall[origin]
        dist = jnp.abs(qpos - kpos + d * tokens).astype(F32) / BLOCK
        for h in range(heads):
            s = dot_t(qs[h], keys) * scale - slopes[h] * dist
            if masked:
                s = s + mask[origin]
            elif first:
                s = jnp.where(kpos // BLOCK <= qpos // BLOCK, s, NEG)
            top = jnp.max(s, axis=1, keepdims=True)
            if not first:
                before = mrun[h][:, :1]
                top = jnp.maximum(top, before)
                fade = jnp.exp(before - top)
            w = jnp.exp(s - top)
            total = jnp.sum(w, axis=1, keepdims=True)
            summed = dot(w.astype(BF16), values)
            if not first:
                total = total + lrun[h][:, :1] * fade
                summed = summed + acc[h] * fade
            mrun[h] = jnp.broadcast_to(top, (tokens, HEAD_DIM))
            lrun[h] = jnp.broadcast_to(total, (tokens, HEAD_DIM))
            acc[h] = summed

    def later(d):
        pl.when(z - d >= 0)(lambda: chunk(d, False))
        step_a(2, d)
        if isinstance(d, int):
            if d > 1:
                step_b(2, d - 1)
        else:
            pl.when(d > 1)(lambda: step_b(2, d - 1))

    chunk(0, True)
    loop(1, n, later)
    step_b(2, n - 1)
    half = tokens // 2
    for h in range(heads):
        value = (acc[h] / lrun[h]).astype(BF16)
        att[:, :, h * HEAD_DIM : (h + 1) * HEAD_DIM] = value.reshape(2, half, HEAD_DIM)

    def out_copy(origin):
        return remote(psend.at[origin], precv.at[origin], osend.at[origin], orecv.at[origin], sib)

    def project_out(origin, weight):
        psend[origin] = dot_t(att[1 - tp], weight).astype(BF16)
        out_copy(origin).start()
        pown[origin] = dot_t(att[tp], weight).astype(BF16)

    project_out(z, wo[...].reshape(rows, -1))
    loop(1, n, lambda d: step_c(2, d))

    def finish(origin):
        out_copy(origin).wait()
        value = pown[origin].astype(F32) + precv[origin].astype(F32)
        first = origin * rows
        if not isinstance(origin, int):
            first = pl.multiple_of(first, rows)
        out[:, pl.ds(first, rows)] = value.astype(BF16)

    finish(z)
    loop(1, n, lambda d: both(d, lambda origin, up: finish(origin)))

    loop(1, n, lambda d: key_each(d, lambda copy: copy.wait_send()))
    for g in range(3):
        for shard in groups[g]:
            @pl.when(z + 1 < n)
            def _():
                along(shard, z, 0, True).wait_send()

            @pl.when(z >= 1)
            def _():
                along(shard, z, 1, True).wait_send()

    def drain(d):
        def body(origin, up):
            for g in range(3):
                for shard in groups[g]:
                    if up:
                        @pl.when(z + 1 < n)
                        def _():
                            along(shard, origin, 0, False).wait_send()
                    else:
                        @pl.when(z >= 1)
                        def _():
                            along(shard, origin, 1, False).wait_send()
                    for kind in (2, 3, 4, 5):
                        across(shard, origin, kind).wait_send()

        both(d, body)

    loop(1, n, drain)


def on_device(n, hidden_in, norm_gain, query_weight, key_weight, value_weight, out_weight, slopes, block_choice):
    _, tokens, half_d = hidden_in.shape
    rows, width = query_weight.shape
    key_width = key_weight.shape[1]
    heads = width // HEAD_DIM
    local_blocks = block_choice.shape[1]
    blocks = n * local_blocks
    masked = blocks > NSEL

    def cut(w):
        return w.reshape(8, rows // 8, w.shape[1])

    operands = [
        hidden_in[0],
        norm_gain.reshape(half_d // 128, 128),
        cut(query_weight),
        cut(key_weight),
        cut(value_weight),
        cut(out_weight),
        slopes,
    ]
    vmem = pl.BlockSpec(memory_space=pltpu.VMEM)
    specs = [vmem] * 6 + [pl.BlockSpec(memory_space=pltpu.SMEM)]
    if masked:
        block = lax.axis_index("kv") * local_blocks + jnp.arange(local_blocks, dtype=jnp.int32)
        slot = jnp.arange(NSEL, dtype=jnp.int32)
        used = slot[None, :] < jnp.minimum(NSEL, block + 1)[:, None]
        names = jnp.arange(blocks, dtype=jnp.int32)
        hit = (block_choice[0][:, :, None] == names[None, None, :]) & used[:, :, None]
        bias = jnp.where(jnp.any(hit, axis=1), 0.0, NEG).astype(F32)
        bias = jnp.repeat(jnp.repeat(bias, BLOCK, axis=0), BLOCK, axis=1)
        operands.append(bias.reshape(tokens, n, tokens).swapaxes(0, 1))
        specs.append(vmem)
    dma = pltpu.SemaphoreType.DMA
    full = (n, 8, rows // 8)
    result = pl.pallas_call(
        functools.partial(kernel, n, masked),
        out_shape=jax.ShapeDtypeStruct((tokens // 2, n * rows), BF16),
        in_specs=specs,
        out_specs=vmem,
        scratch_shapes=[
            pltpu.VMEM((tokens, half_d), BF16),
            pltpu.VMEM((half_d // 128, 128), F32),
            pltpu.VMEM((n, tokens, rows), BF16),
            pltpu.VMEM((*full, width), BF16),
            pltpu.VMEM((*full, key_width), BF16),
            pltpu.VMEM((*full, key_width), BF16),
            pltpu.VMEM((*full, width), BF16),
            pltpu.VMEM((tokens, width), F32),
            pltpu.VMEM((tokens, key_width), F32),
            pltpu.VMEM((tokens, key_width), F32),
            pltpu.VMEM((heads, tokens, HEAD_DIM), BF16),
            pltpu.VMEM((n, tokens, key_width), BF16),
            pltpu.VMEM((n, tokens, key_width), BF16),
            pltpu.VMEM((heads, tokens, HEAD_DIM), F32),
            pltpu.VMEM((heads, tokens, HEAD_DIM), F32),
            pltpu.VMEM((heads, tokens, HEAD_DIM), F32),
            pltpu.VMEM((2, tokens // 2, width), BF16),
            pltpu.VMEM((n, tokens // 2, rows), BF16),
            pltpu.VMEM((n, tokens // 2, rows), BF16),
            pltpu.VMEM((n, tokens // 2, rows), BF16),
            dma((4, 6, n)),
            dma((4, 6, n)),
            dma((2, n)),
            dma((2, n)),
            dma((2,)),
            dma((2,)),
            dma((n,)),
            dma((n,)),
        ],
        compiler_params=pltpu.CompilerParams(collective_id=0, has_side_effects=True),
    )(*operands)
    return result[None]


def solution(mesh):
    in_specs = (
        P(("grp", "dp"), "kv", "tp"),
        P("tp"),
        P("kv", "tp"),
        P("kv", "tp"),
        P("kv", "tp"),
        P("kv", "tp"),
        P("tp"),
        P(("grp", "dp"), "kv", None),
    )
    out_specs = P(("grp", "dp"), ("kv", "tp"), None)
    return jax.shard_map(
        functools.partial(on_device, mesh.shape["kv"]),
        mesh=mesh,
        in_specs=in_specs,
        out_specs=out_specs,
        check_vma=False,
    )
```

time: 151 us -> 61.8 us (0.41)
  blocking collectives: 63.6 us -> 0 us
  Pallas kernels: 0 us -> 58.8 us
  waiting for transfers between devices: 51.1 us -> 0 us
  between operations: 13.2 us -> 0.01 us
  matrix products: 11.7 us -> 0 us
  other arithmetic: 6.49 us -> 0 us
    all_gather x4 -> x0, blocking collectives: 60.8 us -> none  [the longest x1 20.1 us: on_device(): lax.all_gather(value_weight, 'kv', axis=0, tiled=True)]
    pallas_call x0 -> x1, Pallas kernels: none -> 58.8 us  [on_device(): pl.pallas_call(functools.partial(kernel, n, masked), out_shape=jax.ShapeD...]
    all_gather x3 -> x0, waiting for transfers between devices: 39.8 us -> none  [the longest x1 38.4 us: on_device(): out_full = lax.all_gather(out_weight, 'kv', axis=0, tiled=True)]
    dot_general x6 -> x0, matrix products: 11.7 us -> none  [the longest x3 4.45 us: project(): return jnp.dot(rows, weight, preferred_element_type=jnp.float32)]
    reduce_scatter x1 -> x0, waiting for transfers between devices: 9.84 us -> none  [on_device(): lax.psum_scatter(lax.dot_general(piece, out_full, (((1,), (1,)), ((), ())...]
    psum x1 -> x0, blocking collectives: 2.8 us -> none  [on_device(): square_sum = lax.psum(jnp.sum(local * local, axis=1), 'tp')]
    reduce_sum x2 -> x0, other arithmetic: 2.71 us -> none  [the longest x1 1.49 us: on_device(): total = jnp.sum(weights, axis=4)]
    gather x2 -> x0, local copies, waits for them, and re-layouts: 2.44 us -> none  [the longest x1 1.69 us: on_device(): key_sel = key_all.reshape(-1, BLOCK, kv_local, HEAD_DIM)[choice_local]]
  transfers between devices with their start and end apart: 4 -> 0, of which waited for: 3 -> 0; matrix products, arithmetic and copies ran while one was open for 10% -> 0% of each run, Pallas kernels for 0% -> 0%
where the time goes in v1:
time: 61.8 us; the launch traced here: 60.7 us
  Pallas kernels  58.8 us (95%)
  local copies, waits for them, and re-layouts  1.88 us (3%)
    pallas_call x1, Pallas kernels, on_device(): pl.pallas_call(functools.partial(kernel, n, masked), out_shape=jax.ShapeD...  58.8 us
    unnamed x1, local copies, waits for them, and re-layouts  1.88 us

profile of v1, /device:TPU:25, one launch (start us, length us, event | category | flops | bytes accessed | tf_op | source)
XLA Modules:
  0.0 60.7 jit_solution(1993708214399165973)
XLA Ops:
  0.0 58.8 %shard_map.73 = bf16[128,2048]{1,0:T(8,128)(2,1)} custom-call(bf16[256,1024]{1,0:T(8,128)(2,1)} %bitcast.8, f32[8,128]{1,0:T(8,128)} %bitcast.13, bf16[8,64,512]{2,1,0:T(8,128)(2,1)} %bitcast.9, bf16[8,64,128]{2,1,0:T(8,128)(2,1)} %bitcast.11, bf16[8,64,128]{2,1,0:T(8,128)(2,1)} %bitcast.12, bf16[8,64,512]{2,1,0:T(8,128)(2,1)} %bitcast.10, f32[4]{0:T(128)} %refs_6_.1), custom_call_target="tpu_custom_call" | custom-call | tf_op jit(solution)/shard_map/pallas_call | solution.py:379
  58.8 1.9 %copy.9 = bf16[1,128,2048]{2,1,0:T(8,128)(2,1)} copy(bf16[1,128,2048]{2,1,0:T(8,128)(2,1)} %bitcast.7) | data formatting | bytes 1048576

commit v2 on v1

--- a/solution.py
+++ b/solution.py
@@ -12,6 +12,21 @@
 NSEL = 16
 EPS = 1e-06
 NEG = -1e30
+ORDER = (
+    ("own", 1, 1), ("own", 0, -1), ("own", 0, -3), ("norm", 0, 0), ("own", 0, 2), ("pass", 0, -1),
+    ("own", 0, -2), ("own", 0, 1), ("pass", 1, 1), ("own", 0, 3), ("own", 1, -1), ("pass", 0, -2),
+    ("pass", 0, 2), ("pass", 0, -3), ("pass", 0, 1), ("turn", 0, -1), ("pass", 1, -1), ("pass", 0, 3),
+    ("turn", 1, 1), ("turn", 0, 2), ("own", 2, -1), ("turn", 0, 3), ("pass", 1, 2), ("own", 2, 1),
+    ("turn", 0, -2), ("turn", 0, 1), ("pass", 1, 3), ("turn", 0, -3), ("use", 0, -1), ("pass", 1, -2),
+    ("use", 0, 2), ("pass", 2, 1), ("pass", 2, -1), ("use", 0, 1), ("turn", 1, -2), ("pass", 1, -3),
+    ("turn", 1, 3), ("use", 0, 3), ("use", 0, -3), ("use", 1, 1), ("pass", 2, 2), ("turn", 1, 2),
+    ("pass", 2, 3), ("use", 0, -2), ("turn", 1, -1), ("keys", 0, 0), ("pass", 2, -2), ("turn", 1, -3),
+    ("use", 1, 3), ("pass", 2, -3), ("use", 1, -1), ("turn", 2, 2), ("turn", 2, -1), ("turn", 2, 1),
+    ("use", 1, -3), ("use", 1, -2), ("use", 1, 2), ("turn", 2, -2), ("chunk", 0, 0), ("chunk", 0, 1),
+    ("turn", 2, 3), ("chunk", 0, 2), ("chunk", 0, 3), ("turn", 2, -3), ("out", 0, 0), ("use", 2, 3),
+    ("use", 2, 1), ("use", 2, -2), ("use", 2, -1), ("use", 2, 2), ("use", 2, -3),
+)
+ROUTES = ("uni", "chain", "chain")
 MESH = pl.DeviceIdType.MESH
 BF16 = jnp.bfloat16
 F32 = jnp.float32
@@ -41,7 +56,7 @@
     (
         out, hid2, gain2, xn, fq, fk, fv, fo, qacc, kacc, vacc, qs, kall, vall,
         mrun, lrun, acc, att, pown, psend, precv,
-        wsend, wrecv, ksend, krecv, hsend, hrecv, osend, orecv,
+        wsend, wrecv, zsend, ksend, krecv, hsend, hrecv, osend, orecv,
     ) = refs
     grp, dp = lax.axis_index("grp"), lax.axis_index("dp")
     z, tp = lax.axis_index("kv"), lax.axis_index("tp")
@@ -79,12 +94,16 @@
     for copy in swap:
         copy.start()
 
-    def along(shard, origin, kind, own):
+    def along(shard, origin, step, act):
         w, f, a = shard
         part = pl.ds(2 * col, 2)
-        src = w.at[part] if own else f.at[origin, part]
-        dev = at_z(z + 1) if kind == 0 else at_z(z - 1)
-        return remote(src, f.at[origin, part], wsend.at[a, kind, origin], wrecv.at[a, 0, origin], dev)
+        src = w.at[part] if origin is z else f.at[origin, part]
+        target = z + step
+
+        @pl.when((target < n) & (target >= 0))
+        def _():
+            sem = lax.rem(target, n)
+            act(remote(src, f.at[origin, part], zsend.at[a, sem, origin], wrecv.at[a, 0, origin], at_z(target)))
 
     def across(shard, origin, kind):
         _, f, a = shard
@@ -109,43 +128,51 @@
         ref = f.at[origin, part]
         remote(ref, ref, wsend.at[a, kind, origin], wrecv.at[a, kind, origin], x_id).wait_recv()
 
-    def start_own(g):
+    def start(copy):
+        copy.start()
+
+    def own_steps(g):
+        far = {"uni": n - 1, "even": 2, "chain": 1}[ROUTES[g]]
+        return [sign * d for d in range(1, far + 1) for sign in (1, -1)]
+
+    def own(g, step, act):
         for shard in groups[g]:
-            @pl.when(z + 1 < n)
-            def _():
-                along(shard, z, 0, True).start()
-
-            @pl.when(z >= 1)
-            def _():
-                along(shard, z, 1, True).start()
-
-    def both(d, body):
-        @pl.when(z - d >= 0)
-        def _():
-            body(z - d, True)
-
-        @pl.when(z + d < n)
-        def _():
-            body(z + d, False)
-
-    def step_a(g, d):
+            along(shard, z, step, act)
+
+    def forwards(g, shard, origin, up, d, act):
+        def go():
+            for step in (1, 2) if ROUTES[g] == "even" else (1,):
+                along(shard, origin, step if up else -step, act)
+
+        if ROUTES[g] == "chain":
+            go()
+        elif ROUTES[g] == "even":
+            if not isinstance(d, int):
+                pl.when(lax.rem(d, 2) == 0)(go)
+            elif d % 2 == 0:
+                go()
+
+    def one(d, up, body):
+        if up:
+            pl.when(z - d >= 0)(lambda: body(z - d, True))
+        else:
+            pl.when(z + d < n)(lambda: body(z + d, False))
+
+    def both(d, body, ways=(True, False)):
+        for up in ways:
+            one(d, up, body)
+
+    def step_a(g, d, ways=(True, False)):
         def body(origin, up):
             for shard in groups[g]:
                 arrive(shard, origin, 0)
-                if up:
-                    @pl.when(z + 1 < n)
-                    def _():
-                        along(shard, origin, 0, False).start()
-                else:
-                    @pl.when(z >= 1)
-                    def _():
-                        along(shard, origin, 1, False).start()
+                forwards(g, shard, origin, up, d, start)
                 across(shard, origin, 2).start()
                 across(shard, origin, 3).start()
 
-        both(d, body)
-
-    def step_b(g, d):
+        both(d, body, ways)
+
+    def step_b(g, d, ways=(True, False)):
         def body(origin, up):
             for shard in groups[g]:
                 arrive(shard, origin, 2)
@@ -153,12 +180,12 @@
                 arrive(shard, origin, 3)
                 across(shard, origin, 5).start()
 
-        both(d, body)
+        both(d, body, ways)
 
     def whole(f, origin):
         return f[origin].reshape(rows, f.shape[-1])
 
-    def step_c(g, d):
+    def step_c(g, d, ways=(True, False)):
         def body(origin, up):
             for shard in groups[g]:
                 arrive(shard, origin, 4)
@@ -169,31 +196,29 @@
                 else:
                     project_out(origin, whole(fo, origin))
 
-        both(d, body)
-
-    start_own(0)
-    start_own(1)
-
-    for copy in swap:
-        copy.wait()
-    lanes = HEAD_DIM
-    square = jnp.zeros((tokens, lanes), F32)
-    for ref in (hid, hid2):
-        for j in range(half_d // lanes):
-            piece = ref[:, j * lanes : (j + 1) * lanes].astype(F32)
-            square = square + piece * piece
-    inverse = lax.rsqrt(jnp.sum(square, axis=1, keepdims=True) / (2 * half_d) + EPS)
-    for ref, g_ref, half in ((hid, gain, tp), (hid2, gain2, 1 - tp)):
-        for j in range(half_d // lanes):
-            piece = ref[:, j * lanes : (j + 1) * lanes].astype(F32)
-            value = (piece * inverse * g_ref[j : j + 1, :]).astype(BF16)
-            first = j * lanes
-            xn[half * (n // 2) + first // rows, :, first % rows : first % rows + lanes] = value
-
-    mine = xn[z]
-    kacc[...] = dot(mine, wk[...].reshape(rows, -1))
-    vacc[...] = dot(mine, wv[...].reshape(rows, -1))
-    qacc[...] = dot(mine, wq[...].reshape(rows, -1))
+        both(d, body, ways)
+
+    def norm():
+        for copy in swap:
+            copy.wait()
+        lanes = HEAD_DIM
+        square = jnp.zeros((tokens, lanes), F32)
+        for ref in (hid, hid2):
+            for j in range(half_d // lanes):
+                piece = ref[:, j * lanes : (j + 1) * lanes].astype(F32)
+                square = square + piece * piece
+        inverse = lax.rsqrt(jnp.sum(square, axis=1, keepdims=True) / (2 * half_d) + EPS)
+        for ref, g_ref, half in ((hid, gain, tp), (hid2, gain2, 1 - tp)):
+            for j in range(half_d // lanes):
+                piece = ref[:, j * lanes : (j + 1) * lanes].astype(F32)
+                value = (piece * inverse * g_ref[j : j + 1, :]).astype(BF16)
+                first = j * lanes
+                xn[half * (n // 2) + first // rows, :, first % rows : first % rows + lanes] = value
+
+        mine = xn[z]
+        kacc[...] = dot(mine, wk[...].reshape(rows, -1))
+        vacc[...] = dot(mine, wv[...].reshape(rows, -1))
+        qacc[...] = dot(mine, wq[...].reshape(rows, -1))
 
     def key_copy(ref, i, d):
         return remote(ref.at[z], ref.at[z], ksend.at[i, d], krecv.at[i, z], at_z(z + d))
@@ -204,40 +229,10 @@
             for i, ref in enumerate((kall, vall)):
                 act(key_copy(ref, i, d))
 
-    def pipe(d):
-        step_a(0, d)
-        if isinstance(d, int):
-            if d > 1:
-                step_b(0, d - 1)
-            if d > 2:
-                step_c(0, d - 2)
-        else:
-            pl.when(d > 1)(lambda: step_b(0, d - 1))
-            pl.when(d > 2)(lambda: step_c(0, d - 2))
-
-    loop(1, n, pipe)
-    step_a(1, 1)
-    step_b(0, n - 1)
-    step_c(0, n - 2)
-    step_a(1, 2)
-    step_b(1, 1)
-    step_c(0, n - 1)
-    kall[z] = kacc[...].astype(BF16)
-    vall[z] = vacc[...].astype(BF16)
-    loop(1, n, lambda d: key_each(d, lambda copy: copy.start()))
-    start_own(2)
-
-    def pipe_q(d):
-        step_a(1, d)
-        step_b(1, d - 1)
-        step_c(1, d - 2)
-
-    loop(3, n, pipe_q)
-    step_b(1, n - 1)
-    step_c(1, n - 2)
-    step_c(1, n - 1)
-    for h in range(heads):
-        qs[h] = qacc[:, h * HEAD_DIM : (h + 1) * HEAD_DIM].astype(BF16)
+    def send_keys():
+        kall[z] = kacc[...].astype(BF16)
+        vall[z] = vacc[...].astype(BF16)
+        loop(1, n, lambda d: key_each(d, start))
 
     scale = HEAD_DIM**-0.5
     qpos = lax.broadcasted_iota(jnp.int32, (tokens, tokens), 0)
@@ -248,6 +243,9 @@
         if not first:
             for i, ref in enumerate((kall, vall)):
                 remote(ref.at[origin], ref.at[origin], ksend.at[i, d], krecv.at[i, origin], sib).wait_recv()
+        else:
+            for h in range(heads):
+                qs[h] = qacc[:, h * HEAD_DIM : (h + 1) * HEAD_DIM].astype(BF16)
         keys, values = kall[origin], vall[origin]
         dist = jnp.abs(qpos - kpos + d * tokens).astype(F32) / BLOCK
         for h in range(heads):
@@ -271,23 +269,6 @@
             lrun[h] = jnp.broadcast_to(total, (tokens, HEAD_DIM))
             acc[h] = summed
 
-    def later(d):
-        pl.when(z - d >= 0)(lambda: chunk(d, False))
-        step_a(2, d)
-        if isinstance(d, int):
-            if d > 1:
-                step_b(2, d - 1)
-        else:
-            pl.when(d > 1)(lambda: step_b(2, d - 1))
-
-    chunk(0, True)
-    loop(1, n, later)
-    step_b(2, n - 1)
-    half = tokens // 2
-    for h in range(heads):
-        value = (acc[h] / lrun[h]).astype(BF16)
-        att[:, :, h * HEAD_DIM : (h + 1) * HEAD_DIM] = value.reshape(2, half, HEAD_DIM)
-
     def out_copy(origin):
         return remote(psend.at[origin], precv.at[origin], osend.at[origin], orecv.at[origin], sib)
 
@@ -296,8 +277,41 @@
         out_copy(origin).start()
         pown[origin] = dot_t(att[tp], weight).astype(BF16)
 
-    project_out(z, wo[...].reshape(rows, -1))
-    loop(1, n, lambda d: step_c(2, d))
+    def start_out():
+        half = tokens // 2
+        for h in range(heads):
+            value = (acc[h] / lrun[h]).astype(BF16)
+            att[:, :, h * HEAD_DIM : (h + 1) * HEAD_DIM] = value.reshape(2, half, HEAD_DIM)
+        project_out(z, wo[...].reshape(rows, -1))
+
+    def later_chunk(d):
+        pl.when(z - d >= 0)(lambda: chunk(d, False))
+
+    if n == 4:
+        for step, g, d in ORDER:
+            if step == "own":
+                own(g, d, start)
+            elif step in ("pass", "turn", "use"):
+                {"pass": step_a, "turn": step_b, "use": step_c}[step](g, abs(d), (d > 0,))
+            elif step == "chunk":
+                later_chunk(d) if d else chunk(0, True)
+            else:
+                {"norm": norm, "keys": send_keys, "out": start_out}[step]()
+    else:
+        for g in range(3):
+            for step in own_steps(g):
+                own(g, step, start)
+        norm()
+        for g, then in ((0, send_keys), (1, lambda: chunk(0, True))):
+            loop(1, n, lambda d: step_a(g, d))
+            loop(1, n, lambda d: step_b(g, d))
+            loop(1, n, lambda d: step_c(g, d))
+            then()
+        loop(1, n, lambda d: step_a(2, d))
+        loop(1, n, lambda d: step_b(2, d))
+        loop(1, n, later_chunk)
+        start_out()
+        loop(1, n, lambda d: step_c(2, d))
 
     def finish(origin):
         out_copy(origin).wait()
@@ -310,29 +324,19 @@
     finish(z)
     loop(1, n, lambda d: both(d, lambda origin, up: finish(origin)))
 
-    loop(1, n, lambda d: key_each(d, lambda copy: copy.wait_send()))
+    def left(copy):
+        copy.wait_send()
+
+    loop(1, n, lambda d: key_each(d, left))
     for g in range(3):
-        for shard in groups[g]:
-            @pl.when(z + 1 < n)
-            def _():
-                along(shard, z, 0, True).wait_send()
-
-            @pl.when(z >= 1)
-            def _():
-                along(shard, z, 1, True).wait_send()
+        for step in own_steps(g):
+            own(g, step, left)
 
     def drain(d):
         def body(origin, up):
             for g in range(3):
                 for shard in groups[g]:
-                    if up:
-                        @pl.when(z + 1 < n)
-                        def _():
-                            along(shard, origin, 0, False).wait_send()
-                    else:
-                        @pl.when(z >= 1)
-                        def _():
-                            along(shard, origin, 1, False).wait_send()
+                    forwards(g, shard, origin, up, d, left)
                     for kind in (2, 3, 4, 5):
                         across(shard, origin, kind).wait_send()
 
@@ -404,6 +408,7 @@
             pltpu.VMEM((n, tokens // 2, rows), BF16),
             dma((4, 6, n)),
             dma((4, 6, n)),
+            dma((4, n, n)),
             dma((2, n)),
             dma((2, n)),
             dma((2,)),

time: 61.8 us -> 56 us (0.906); the launches traced: 60.7 us -> 55.8 us
  Pallas kernels: 58.8 us -> 53.9 us
    pallas_call x1, Pallas kernels: 58.8 us -> 53.9 us  [on_device(): pl.pallas_call(functools.partial(kernel, n, masked), out_shape=jax.ShapeD...]
where the time goes in v2:
time: 56 us; the launch traced here: 55.8 us
  Pallas kernels  53.9 us (96%)
  local copies, waits for them, and re-layouts  1.88 us (3%)
    pallas_call x1, Pallas kernels, on_device(): pl.pallas_call(functools.partial(kernel, n, masked), out_shape=jax.ShapeD...  53.9 us
    unnamed x1, local copies, waits for them, and re-layouts  1.88 us

profile of v2, /device:TPU:25, one launch (start us, length us, event | category | flops | bytes accessed | tf_op | source)
XLA Modules:
  0.0 55.8 jit_solution(14117927649318553131)
XLA Ops:
  0.0 53.9 %shard_map.73 = bf16[128,2048]{1,0:T(8,128)(2,1)} custom-call(bf16[256,1024]{1,0:T(8,128)(2,1)} %bitcast.8, f32[8,128]{1,0:T(8,128)} %bitcast.13, bf16[8,64,512]{2,1,0:T(8,128)(2,1)} %bitcast.9, bf16[8,64,128]{2,1,0:T(8,128)(2,1)} %bitcast.11, bf16[8,64,128]{2,1,0:T(8,128)(2,1)} %bitcast.12, bf16[8,64,512]{2,1,0:T(8,128)(2,1)} %bitcast.10, f32[4]{0:T(128)} %refs_6_.1), custom_call_target="tpu_custom_call" | custom-call | tf_op jit(solution)/shard_map/pallas_call | solution.py:383
  53.9 1.9 %copy.9 = bf16[1,128,2048]{2,1,0:T(8,128)(2,1)} copy(bf16[1,128,2048]{2,1,0:T(8,128)(2,1)} %bitcast.7) | data formatting | bytes 1048576

commit v3 on v2

--- a/solution.py
+++ b/solution.py
@@ -13,20 +13,20 @@
 EPS = 1e-06
 NEG = -1e30
 ORDER = (
-    ("own", 1, 1), ("own", 0, -1), ("own", 0, -3), ("norm", 0, 0), ("own", 0, 2), ("pass", 0, -1),
-    ("own", 0, -2), ("own", 0, 1), ("pass", 1, 1), ("own", 0, 3), ("own", 1, -1), ("pass", 0, -2),
-    ("pass", 0, 2), ("pass", 0, -3), ("pass", 0, 1), ("turn", 0, -1), ("pass", 1, -1), ("pass", 0, 3),
-    ("turn", 1, 1), ("turn", 0, 2), ("own", 2, -1), ("turn", 0, 3), ("pass", 1, 2), ("own", 2, 1),
-    ("turn", 0, -2), ("turn", 0, 1), ("pass", 1, 3), ("turn", 0, -3), ("use", 0, -1), ("pass", 1, -2),
-    ("use", 0, 2), ("pass", 2, 1), ("pass", 2, -1), ("use", 0, 1), ("turn", 1, -2), ("pass", 1, -3),
-    ("turn", 1, 3), ("use", 0, 3), ("use", 0, -3), ("use", 1, 1), ("pass", 2, 2), ("turn", 1, 2),
-    ("pass", 2, 3), ("use", 0, -2), ("turn", 1, -1), ("keys", 0, 0), ("pass", 2, -2), ("turn", 1, -3),
-    ("use", 1, 3), ("pass", 2, -3), ("use", 1, -1), ("turn", 2, 2), ("turn", 2, -1), ("turn", 2, 1),
-    ("use", 1, -3), ("use", 1, -2), ("use", 1, 2), ("turn", 2, -2), ("chunk", 0, 0), ("chunk", 0, 1),
-    ("turn", 2, 3), ("chunk", 0, 2), ("chunk", 0, 3), ("turn", 2, -3), ("out", 0, 0), ("use", 2, 3),
-    ("use", 2, 1), ("use", 2, -2), ("use", 2, -1), ("use", 2, 2), ("use", 2, -3),
+    ("own", 0, -1), ("own", 1, -1), ("own", 0, 1), ("own", 1, 1), ("pass", 0, -1), ("pass", 0, 1),
+    ("pass", 0, -2), ("pass", 1, 1), ("pass", 1, -1), ("norm", 0, 0), ("own", 2, 1), ("own", 2, -1),
+    ("pass", 0, 2), ("turn", 0, -1), ("pass", 0, -3), ("turn", 0, 1), ("pass", 1, 2), ("turn", 0, 2),
+    ("turn", 0, -2), ("pass", 2, 1), ("pass", 1, -2), ("turn", 0, -3), ("turn", 1, -1), ("pass", 0, 3),
+    ("use", 0, -1), ("pass", 2, -1), ("pass", 1, -3), ("use", 0, 1), ("use", 0, 2), ("use", 0, -2),
+    ("pass", 1, 3), ("turn", 0, 3), ("turn", 1, 2), ("turn", 1, 1), ("turn", 1, 3), ("pass", 2, 2),
+    ("use", 0, 3), ("pass", 2, 3), ("use", 0, -3), ("pass", 2, -2), ("keys", 0, 0), ("turn", 1, -2),
+    ("turn", 1, -3), ("use", 1, 1), ("pass", 2, -3), ("turn", 2, -1), ("use", 1, 2), ("use", 1, -3),
+    ("use", 1, -1), ("turn", 2, -2), ("use", 1, -2), ("turn", 2, 1), ("use", 1, 3), ("chunk", 0, 0),
+    ("chunk", 0, 1), ("turn", 2, 2), ("turn", 2, 3), ("chunk", 0, 2), ("turn", 2, -3), ("chunk", 0, 3),
+    ("out", 0, 0), ("use", 2, 1), ("use", 2, -2), ("use", 2, -1), ("use", 2, 3), ("use", 2, 2),
+    ("use", 2, -3),
 )
-ROUTES = ("uni", "chain", "chain")
+ROUTES = ("chain", "chain", "chain")
 MESH = pl.DeviceIdType.MESH
 BF16 = jnp.bfloat16
 F32 = jnp.float32

time: 56 us -> 52.9 us (0.945)
  Pallas kernels: 53.9 us -> 50.8 us
    pallas_call x1, Pallas kernels: 53.9 us -> 50.8 us  [on_device(): pl.pallas_call(functools.partial(kernel, n, masked), out_shape=jax.ShapeD...]
where the time goes in v3:
time: 52.9 us; the launch traced here: 52.7 us
  Pallas kernels  50.8 us (96%)
  local copies, waits for them, and re-layouts  1.88 us (4%)
    pallas_call x1, Pallas kernels, on_device(): pl.pallas_call(functools.partial(kernel, n, masked), out_shape=jax.ShapeD...  50.8 us
    unnamed x1, local copies, waits for them, and re-layouts  1.88 us

profile of v3, /device:TPU:25, one launch (start us, length us, event | category | flops | bytes accessed | tf_op | source)
XLA Modules:
  0.0 52.7 jit_solution(15130350052359761091)
XLA Ops:
  0.0 50.8 %shard_map.73 = bf16[128,2048]{1,0:T(8,128)(2,1)} custom-call(bf16[256,1024]{1,0:T(8,128)(2,1)} %bitcast.8, f32[8,128]{1,0:T(8,128)} %bitcast.13, bf16[8,64,512]{2,1,0:T(8,128)(2,1)} %bitcast.9, bf16[8,64,128]{2,1,0:T(8,128)(2,1)} %bitcast.11, bf16[8,64,128]{2,1,0:T(8,128)(2,1)} %bitcast.12, bf16[8,64,512]{2,1,0:T(8,128)(2,1)} %bitcast.10, f32[4]{0:T(128)} %refs_6_.1), custom_call_target="tpu_custom_call" | custom-call | tf_op jit(solution)/shard_map/pallas_call | solution.py:383
  50.8 1.9 %copy.9 = bf16[1,128,2048]{2,1,0:T(8,128)(2,1)} copy(bf16[1,128,2048]{2,1,0:T(8,128)(2,1)} %bitcast.7) | data formatting | bytes 1048576
